TPU v7x, 512 devices: a whole 4x4x16 slice. The times are simulated.
512 devices in a mesh: ep: 32 (over z, core), tp: 16 (over y, x).
Axes of the slice: x: 4, y: 4, z: 16, core: 2. Of those that a mesh axis runs over, the one named last changes fastest.
Arguments:
- tokens: bfloat16 [4096, 2048], P('ep'), may hold values from -6 to 6
- selected: int32 [32, 1024], P(None, 'ep'), may hold values from -1 to 127, as said below
- affinity: float32 [32, 1024], P(None, 'ep'), may hold values from 0.05 to 1
- w_gate: bfloat16 [32, 2048, 2048], P('ep', None, 'tp'), may hold values from -0.125 to 0.125
- w_up: bfloat16 [32, 2048, 2048], P('ep', None, 'tp'), may hold values from -0.125 to 0.125
- w_down: bfloat16 [32, 2048, 2048], P('ep', 'tp'), may hold values from -0.125 to 0.125
Outputs:
- combined: bfloat16 [4096, 2048], P('ep', 'tp')
Inputs may be any that keep to these rules, and one draw needn't show every extreme that they name: `selected`: row e holds 32 aligned groups of 32 entries; the live entries of group j are distinct positions within the j-th block of 128 tokens, stand at the front of the group and are followed by -1; each row has 512 live entries in all, the number in a group varies, and some group of every row is full.
All inputs are finite; a program needn't handle non-finite values.
Results may differ from a plain program's by a relative error of at most 0.015.
Values may be sent and summed in bfloat16 or wider, within the bound.
A program may use at most 64 MiB of HBM per device.

v0:
```python
import jax
import jax.numpy as jnp
from jax import lax
from jax.sharding import Mesh
from jax.sharding import PartitionSpec as P

EP = ("ep_0", "ep_1")


def in_blocks(array, dim, peers):
    dims = array.shape
    parts = array.reshape(*dims[:dim], peers, dims[dim] // peers, *dims[dim + 1 :])
    return jnp.moveaxis(parts, dim, 0)


def joined_along(parts, dim):
    dims = list(parts.shape[1:])
    dims[dim] *= parts.shape[0]
    return jnp.moveaxis(parts, 0, dim).reshape(dims)


def moved_by_axis(parts, axes, order):
    dims = [lax.axis_size(a) for a in axes]
    parts = parts.reshape(*dims, *parts.shape[1:])
    for k in order:
        parts = lax.all_to_all(parts, axes[k], split_axis=k, concat_axis=k, tiled=True)
    return parts.reshape(-1, *parts.shape[len(axes) :])


def two_step_exchange(array, groups, order, split_dim, concat_dim):
    peers = lax.axis_size(groups[0]) * lax.axis_size(groups[1])
    parts = in_blocks(array, split_dim, peers)
    return joined_along(moved_by_axis(parts, groups, order), concat_dim)


def sent_to_all(array, axis):
    peers = lax.axis_size(axis)
    return lax.all_to_all(
        jnp.broadcast_to(array[None], (peers, *array.shape)), axis, 0, 0, tiled=True
    )


def gather_directly(array, axis, dim):
    parts = sent_to_all(array, axis)
    return joined_along(parts, dim)


def summed_on_arrival(array, axis, dim):
    peers = lax.axis_size(axis)
    parts = lax.all_to_all(in_blocks(array, dim, peers), axis, 0, 0, tiled=True)
    return jnp.sum(parts.astype(jnp.float32), axis=0)


def per_device(tokens, selected, affinity, w_gate, w_up, w_down):
    ep_count = lax.axis_size(EP)
    tp_count = lax.axis_size("tp")
    local_tokens = tokens.shape[0]
    width = tokens.shape[1]
    experts_here = w_gate.shape[0]
    slot_count = selected.shape[1]
    clamped = jnp.maximum(selected, 0)
    gathered = jnp.take(tokens, clamped, axis=0)
    column_span = width // tp_count
    slab = lax.dynamic_slice_in_dim(gathered, lax.axis_index("tp") * column_span, column_span, 2)
    arrived = two_step_exchange(slab, ("ep_0", "ep_1"), (1, 0), 0, 1)
    segment = gather_directly(arrived, "tp", 2)
    gate_more = jnp.einsum("ecd,edf->ecf", segment, w_gate, preferred_element_type=jnp.float32)
    up_more = jnp.einsum("ecd,edf->ecf", segment, w_up, preferred_element_type=jnp.float32)
    hidden = (jax.nn.silu(gate_more) * up_more).astype(jnp.bfloat16)
    summed = summed_on_arrival(
        jnp.einsum("efd,ecf->dec", w_down, hidden, preferred_element_type=jnp.float32).astype(
            jnp.bfloat16
        ),
        "tp",
        0,
    ).astype(jnp.bfloat16)
    summed = summed.reshape(summed.shape[0], experts_here, ep_count, slot_count)
    returned = lax.all_to_all(summed, EP, split_axis=2, concat_axis=1, tiled=True)
    feature_cols = returned.shape[0]
    returned = returned.reshape(feature_cols, experts_here * ep_count * slot_count)
    weights = jnp.where(selected >= 0, affinity, jnp.zeros_like(affinity)).reshape(-1)
    scaled_rows = returned.astype(jnp.float32).T * weights[:, None]
    combined = (
        jnp.zeros((local_tokens, feature_cols), jnp.float32)
        .at[clamped.reshape(-1)]
        .add(scaled_rows)
    )
    return combined.astype(jnp.bfloat16)


def solution(mesh):
    torus = Mesh(mesh.devices.reshape(16, 2, mesh.shape["tp"]), ("ep_0", "ep_1", "tp"))
    in_specs = (
        P(EP, None),
        P(None, EP),
        P(None, EP),
        P(EP, None, "tp"),
        P(EP, None, "tp"),
        P(EP, "tp", None),
    )
    out_specs = P(EP, "tp")
    return jax.shard_map(
        per_device, mesh=torus, in_specs=in_specs, out_specs=out_specs, check_vma=False
    )
```

profile of v0, /device:TPU:1, one launch (start us, length us, event | category | flops | bytes accessed | tf_op | source)
XLA Modules:
  0.0 214.2 jit_solution(5828575752059299651)
XLA Ops:
  0.0 0.0 copy-start
  0.0 0.8 broadcast_maximum_fusion
  0.8 0.7 broadcast_compare_fusion
  1.5 0.1 reshape.94
  1.6 0.0 copy-done
  1.6 6.0 %gather_fusion = bf16[1024,2048]{1,0:T(8,128)(2,1)} fusion(bf16[128,2048]{1,0:T(8,128)(2,1)S(1)} %copy-done, s32[1024]{0:T(1024)S(1)} %broadcast_clamp_fusion), kind=kCustom, calls=%fused_computation | custom fusion | bytes 8392704 | tf_op jit(solution)/shard_map/jit(_take)/gather | solution.py:62
  7.6 1.1 dynamic-slice_select_fusion
  8.8 10.4 %all_to_all.29 = bf16[16,2,1,32,128]{4,3,0,2,1:T(8,128)(2,1)S(1)} all-to-all(bf16[16,2,1,32,128]{4,3,0,2,1:T(8,128)(2,1)S(1)} %copy.8), channel_id=1, replica_groups=mesh['ep_0'=16,'ep_1'=2,'tp'=16] {'ep_1'}, dimensions={1} | all-to-all | bytes 524288 | tf_op jit(solution)/shard_map/all_to_all | solution.py:26
  19.2 23.4 %all_to_all.30 = bf16[16,2,1,32,128]{4,3,1,2,0:T(8,128)(2,1)S(1)} all-to-all(bf16[16,2,1,32,128]{4,3,1,2,0:T(8,128)(2,1)S(1)} %copy.9), channel_id=1, replica_groups=mesh['ep_0'=16,'ep_1'=2,'tp'=16] {'ep_0'}, dimensions={0} | all-to-all | bytes 524288 | tf_op jit(solution)/shard_map/all_to_all | solution.py:26
  42.6 0.1 copy.10
  42.7 0.5 broadcast_in_dim.31
  43.3 0.0 copy-start.2
  43.3 53.3 %all_to_all.31 = bf16[16,1,1024,128]{2,3,1,0:T(8,128)(2,1)S(1)} all-to-all(bf16[16,1,1024,128]{2,3,1,0:T(8,128)(2,1)S(1)} %broadcast_in_dim.31), channel_id=1, replica_groups=mesh['ep_0'=16,'ep_1'=2,'tp'=16] {'tp'}, dimensions={0} | all-to-all | bytes 8388608 | tf_op jit(solution)/shard_map/all_to_all | solution.py:38
  96.6 0.0 copy-start.1
  96.6 0.0 copy-start.3
  96.6 0.0 copy-start.4
  96.6 1.9 copy-done.1
  98.6 0.0 copy-done.2
  98.6 1.3 fusion.7
  99.8 0.0 copy-done.3
  99.8 0.0 copy-done.4
  99.9 8.5 %convert_bitcast_fusion = bf16[1,128,16,8,128]{4,3,2,1,0:T(8,128)(2,1)} fusion(bf16[1024,2048]{0,1:T(8,128)(2,1)} %bitcast.36, bf16[1,128,2048]{2,1,0:T(8,128)(2,1)S(1)} %copy-done.3, bf16[1,2048,128]{2,1,0:T(8,128)(2,1)S(1)} %copy-done.4, f32[1024,128]{1,0:T(8,128)S(1)} %fusion.7), kind=kOutput, calls=%fused_computation.3 | convolution fusion | flops 1076625408 | bytes 9961472 | tf_op jit(solution)/shard_map/efd,ecf->dec/dot_general | solution.py:71
  108.4 3.3 %copy.15 = bf16[1,128,16,8,128]{4,3,1,0,2:T(8,128)(2,1)S(1)} copy(bf16[1,128,16,8,128]{4,3,2,1,0:T(8,128)(2,1)} %convert_bitcast_fusion) | data formatting | bytes 8388608 | tf_op jit(solution)/shard_map/reshape | solution.py:12
  111.6 47.9 %all_to_all.32 = bf16[16,128,1,1024]{1,3,2,0:T(8,128)(2,1)} all-to-all(bf16[16,128,1,1024]{1,3,2,0:T(8,128)(2,1)S(1)} %bitcast.37), channel_id=1, replica_groups=mesh['ep_0'=16,'ep_1'=2,'tp'=16] {'tp'}, dimensions={0} | all-to-all | bytes 8388608 | tf_op jit(solution)/shard_map/all_to_all | solution.py:50
  159.6 0.0 copy-start.5
  159.6 0.0 copy-start.6
  159.6 3.5 %reduce_sum.12 = bf16[128,1024]{0,1:T(8,128)(2,1)} reduce(bf16[16,128,1,1024]{1,3,2,0:T(8,128)(2,1)} %all_to_all.32, bf16[]{:T(256)} %constant.37.clone.1), dimensions={0,2}, to_apply=%region_0.1 | reduce | flops 1966080 | bytes 4456450 | tf_op jit(solution)/shard_map/reduce_sum | solution.py:51
  163.1 21.3 %all-to-all-start.4 = ((bf16[128,1,32,32]{0,3,1,2:T(8,128)(2,1)}), bf16[128,1,32,32]{0,3,1,2:T(8,128)(2,1)S(1)}, u32[]{:S(2)}, u32[]{:S(2)}) async-start(bf16[128,1,32,32]{0,3,1,2:T(8,128)(2,1)} %bitcast.14), calls=%async_computation.4 | async-start | bytes 524288 | tf_op jit(solution)/shard_map/all_to_all | solution.py:78
  184.5 0.1 reshape.84
  184.5 0.0 copy-done.5
  184.5 0.0 copy-done.6
  184.6 0.1 mul.28
  184.6 22.1 %all-to-all-done.4 = bf16[128,1,32,32]{0,3,1,2:T(8,128)(2,1)S(1)} async-done(((bf16[128,1,32,32]{0,3,1,2:T(8,128)(2,1)}), bf16[128,1,32,32]{0,3,1,2:T(8,128)(2,1)S(1)}, u32[]{:S(2)}, u32[]{:S(2)}) %all-to-all-start.4) | async-done | bytes 262176 | tf_op jit(solution)/shard_map/all_to_all | solution.py:78
  206.7 6.9 %scatter_custom_fusion = f32[128,128]{1,0:T(8,128)S(1)} fusion(s32[1024]{0:T(1024)S(1)} %bitcast.42, bf16[128,1024]{0,1:T(8,128)(2,1)S(1)} %bitcast.40, f32[1024]{0:T(1024)S(1)} %mul.28, f32[]{:T(128)} %constant.11.clone.1), kind=kCustom, calls=%fused_computation.8 | custom fusion | flops 393216 | bytes 331780 | tf_op jit(solution)/shard_map/scatter-add | solution.py:86
  213.6 0.6 convert_element_type.30
  (5 shorter events, 0.1 us)
Async XLA Ops:
  0.0 1.6 copy-start
  43.3 55.3 %copy-start.2 = (bf16[1,2048,128]{2,1,0:T(8,128)(2,1)S(1)}, bf16[1,2048,128]{2,1,0:T(8,128)(2,1)}, u32[]{:S(2)}) copy-start(bf16[1,2048,128]{2,1,0:T(8,128)(2,1)} %param.9) | copy-start | bytes 1572868
  96.6 1.9 copy-start.1
  96.6 3.2 %copy-start.3 = (bf16[1,128,2048]{2,1,0:T(8,128)(2,1)S(1)}, bf16[1,128,2048]{2,1,0:T(8,128)(2,1)}, u32[]{:S(2)}) copy-start(bf16[1,128,2048]{2,1,0:T(8,128)(2,1)} %param.11) | copy-start | bytes 1572868
  96.6 3.2 %copy-start.4 = (bf16[1,2048,128]{2,1,0:T(8,128)(2,1)S(1)}, bf16[1,2048,128]{2,1,0:T(8,128)(2,1)}, u32[]{:S(2)}) copy-start(bf16[1,2048,128]{2,1,0:T(8,128)(2,1)} %param.10) | copy-start | bytes 1572868
  159.6 25.0 %copy-start.5 = (s32[32,32]{1,0:T(8,128)S(1)}, s32[32,32]{1,0:T(8,128)}, u32[]{:S(2)}) copy-start(s32[32,32]{1,0:T(8,128)} %param.7) | copy-start | bytes 12292
  159.6 25.0 %copy-start.6 = (f32[32,32]{1,0:T(8,128)S(1)}, f32[32,32]{1,0:T(8,128)}, u32[]{:S(2)}) copy-start(f32[32,32]{1,0:T(8,128)} %param.8) | copy-start | bytes 12292
  163.1 43.6 %all-to-all-start.4 = ((bf16[128,1,32,32]{0,3,1,2:T(8,128)(2,1)}), bf16[128,1,32,32]{0,3,1,2:T(8,128)(2,1)S(1)}, u32[]{:S(2)}, u32[]{:S(2)}) async-start(bf16[128,1,32,32]{0,3,1,2:T(8,128)(2,1)} %bitcast.14), calls=%async_computation.4 | async-start | bytes 524288 | tf_op jit(solution)/shard_map/all_to_all | solution.py:78
where the time goes:
time: 215 us; the launch traced here: 214 us
  blocking collectives  135 us (63%)
  waiting for transfers between devices  22.1 us (10%)
  starting transfers between devices  21.3 us (10%)
  other arithmetic  13.7 us (6%)
  local copies, waits for them, and re-layouts  12.1 us (6%)
  matrix products  9.8 us (5%)
    all_to_all x1, blocking collectives, sent_to_all(): lax.all_to_all(jnp.broadcast_to(array[None], (peers, *array.shape)), axis...  53.3 us
    all_to_all x1, blocking collectives, summed_on_arrival(): parts = lax.all_to_all(in_blocks(array, dim, peers), axis, 0, 0, tiled=True)  47.9 us
    all_to_all x2, blocking collectives, moved_by_axis(): lax.all_to_all(parts, axes[k], split_axis=k, concat_axis=k, tiled=True)  33.8 us
    all_to_all x1, waiting for transfers between devices, per_device(): lax.all_to_all(summed, EP, split_axis=2, concat_axis=1, tiled=True)  22.1 us
    all_to_all x1, starting transfers between devices, per_device(): lax.all_to_all(summed, EP, split_axis=2, concat_axis=1, tiled=True)  21.3 us
    dot_general x1, matrix products, per_device(): jnp.einsum('efd,ecf->dec', w_down, hidden, preferred_element_type=jnp.flo...  8.52 us
    scatter-add x1, other arithmetic, per_device(): combined = jnp.zeros((local_tokens, feature_cols), jnp.float32).at[clampe...  6.86 us
    gather x1, local copies, waits for them, and re-layouts, per_device(): gathered = jnp.take(tokens, clamped, axis=0)  5.98 us
  transfers between devices with their start and end apart: 1, of which 1 were waited for; matrix products, arithmetic and copies ran while one was open for 0% of the time, Pallas kernels for 0%

commit v1 on v0

--- a/solution.py
+++ b/solution.py
@@ -75,7 +75,9 @@
         0,
     ).astype(jnp.bfloat16)
     summed = summed.reshape(summed.shape[0], experts_here, ep_count, slot_count)
-    returned = lax.all_to_all(summed, EP, split_axis=2, concat_axis=1, tiled=True)
+    shards = jnp.split(summed, lax.axis_size(EP), axis=2)
+    incoming = lax.all_to_all(jnp.stack(shards), EP, 0, 0)
+    returned = jnp.concatenate(incoming, axis=1)
     feature_cols = returned.shape[0]
     returned = returned.reshape(feature_cols, experts_here * ep_count * slot_count)
     weights = jnp.where(selected >= 0, affinity, jnp.zeros_like(affinity)).reshape(-1)

time: 215 us -> 233 us (1.084)
  local copies, waits for them, and re-layouts: 12.1 us -> 31.2 us
    unnamed x14 -> x45, local copies, waits for them, and re-layouts: 1.96 us -> 20.4 us
where the time goes in v1:
time: 233 us; the launch traced here: 232 us
  blocking collectives  135 us (58%)
  local copies, waits for them, and re-layouts  31.2 us (13%)
  waiting for transfers between devices  22.1 us (9%)
  starting transfers between devices  21.3 us (9%)
  other arithmetic  12.7 us (5%)
  matrix products  9.8 us (4%)
    all_to_all x1, blocking collectives, sent_to_all(): lax.all_to_all(jnp.broadcast_to(array[None], (peers, *array.shape)), axis...  53.3 us
    all_to_all x1, blocking collectives, summed_on_arrival(): parts = lax.all_to_all(in_blocks(array, dim, peers), axis, 0, 0, tiled=True)  47.9 us
    all_to_all x2, blocking collectives, moved_by_axis(): lax.all_to_all(parts, axes[k], split_axis=k, concat_axis=k, tiled=True)  33.8 us
    all_to_all x1, waiting for transfers between devices, per_device(): incoming = lax.all_to_all(jnp.stack(shards), EP, 0, 0)  22.1 us
    all_to_all x1, starting transfers between devices, per_device(): incoming = lax.all_to_all(jnp.stack(shards), EP, 0, 0)  21.3 us
    unnamed x45, local copies, waits for them, and re-layouts  20.4 us
    dot_general x1, matrix products, per_device(): jnp.einsum('efd,ecf->dec', w_down, hidden, preferred_element_type=jnp.flo...  8.52 us
    scatter-add x1, other arithmetic, per_device(): combined = jnp.zeros((local_tokens, feature_cols), jnp.float32).at[clampe...  6.38 us
  transfers between devices with their start and end apart: 1, of which 1 were waited for; matrix products, arithmetic and copies ran while one was open for 0% of the time, Pallas kernels for 0%

profile of v1, /device:TPU:1, one launch (start us, length us, event | category | flops | bytes accessed | tf_op | source)
XLA Modules:
  0.0 232.3 jit_solution(8446147504871114239)
XLA Ops:
  0.0 0.0 copy-start
  0.0 0.8 broadcast_compare_fusion
  0.8 0.7 broadcast_maximum_fusion
  1.5 0.1 reshape.90
  1.6 0.0 copy-done
  1.6 6.0 %gather_fusion = bf16[1024,2048]{1,0:T(8,128)(2,1)} fusion(bf16[128,2048]{1,0:T(8,128)(2,1)S(1)} %copy-done, s32[1024]{0:T(1024)S(1)} %broadcast_clamp_fusion), kind=kCustom, calls=%fused_computation | custom fusion | bytes 8392704 | tf_op jit(solution)/shard_map/jit(_take)/gather | solution.py:62
  7.6 1.1 dynamic-slice_select_fusion
  8.8 10.4 %all_to_all.25 = bf16[16,2,1,32,128]{4,3,0,2,1:T(8,128)(2,1)S(1)} all-to-all(bf16[16,2,1,32,128]{4,3,0,2,1:T(8,128)(2,1)S(1)} %copy.101), channel_id=1, replica_groups=mesh['ep_0'=16,'ep_1'=2,'tp'=16] {'ep_1'}, dimensions={1} | all-to-all | bytes 524288 | tf_op jit(solution)/shard_map/all_to_all | solution.py:26
  19.2 23.4 %all_to_all.26 = bf16[16,2,1,32,128]{4,3,1,2,0:T(8,128)(2,1)S(1)} all-to-all(bf16[16,2,1,32,128]{4,3,1,2,0:T(8,128)(2,1)S(1)} %copy.102), channel_id=1, replica_groups=mesh['ep_0'=16,'ep_1'=2,'tp'=16] {'ep_0'}, dimensions={0} | all-to-all | bytes 524288 | tf_op jit(solution)/shard_map/all_to_all | solution.py:26
  42.6 0.1 copy.103
  42.7 0.5 broadcast_in_dim.31
  43.3 0.0 copy-start.2
  43.3 53.3 %all_to_all.27 = bf16[16,1,1024,128]{2,3,1,0:T(8,128)(2,1)S(1)} all-to-all(bf16[16,1,1024,128]{2,3,1,0:T(8,128)(2,1)S(1)} %broadcast_in_dim.31), channel_id=1, replica_groups=mesh['ep_0'=16,'ep_1'=2,'tp'=16] {'tp'}, dimensions={0} | all-to-all | bytes 8388608 | tf_op jit(solution)/shard_map/all_to_all | solution.py:38
  96.6 0.0 copy-start.1
  96.6 1.9 copy-done.1
  98.6 0.0 copy-done.2
  98.6 1.3 fusion.6
  99.8 0.0 copy-done.3
  99.8 0.0 copy-done.4
  99.9 8.5 %convert_bitcast_fusion = bf16[1,128,16,8,128]{4,3,2,1,0:T(8,128)(2,1)} fusion(bf16[1024,2048]{0,1:T(8,128)(2,1)} %bitcast.166, bf16[1,128,2048]{2,1,0:T(8,128)(2,1)S(1)} %copy-done.3, bf16[1,2048,128]{2,1,0:T(8,128)(2,1)S(1)} %copy-done.4, f32[1024,128]{1,0:T(8,128)S(1)} %fusion.6), kind=kOutput, calls=%fused_computation.3 | convolution fusion | flops 1076625408 | bytes 9961472 | tf_op jit(solution)/shard_map/efd,ecf->dec/dot_general | solution.py:71
  108.4 3.3 %copy.108 = bf16[1,128,16,8,128]{4,3,1,0,2:T(8,128)(2,1)S(1)} copy(bf16[1,128,16,8,128]{4,3,2,1,0:T(8,128)(2,1)} %convert_bitcast_fusion) | data formatting | bytes 8388608 | tf_op jit(solution)/shard_map/reshape | solution.py:12
  111.6 47.9 %all_to_all.28 = bf16[16,128,1,1024]{1,3,2,0:T(8,128)(2,1)} all-to-all(bf16[16,128,1,1024]{1,3,2,0:T(8,128)(2,1)S(1)} %bitcast.167), channel_id=1, replica_groups=mesh['ep_0'=16,'ep_1'=2,'tp'=16] {'tp'}, dimensions={0} | all-to-all | bytes 8388608 | tf_op jit(solution)/shard_map/all_to_all | solution.py:50
  159.6 2.9 %reduce_sum.12 = bf16[128,1024]{0,1:T(8,128)(2,1)S(1)} reduce(bf16[16,128,1,1024]{1,3,2,0:T(8,128)(2,1)} %all_to_all.28, bf16[]{:T(256)} %constant.37.clone.1), dimensions={0,2}, to_apply=%region_0.1 | reduce | flops 1966080 | bytes 4456450 | tf_op jit(solution)/shard_map/reduce_sum | solution.py:51
  162.5 0.6 constant_dynamic-update-slice_fusion.31
  163.1 0.6 constant_dynamic-update-slice_fusion.30
  163.6 0.6 constant_dynamic-update-slice_fusion.29
  164.2 0.6 constant_dynamic-update-slice_fusion.28
  164.8 0.6 constant_dynamic-update-slice_fusion.27
  165.4 0.6 constant_dynamic-update-slice_fusion.26
  166.0 0.6 constant_dynamic-update-slice_fusion.25
  166.6 0.6 constant_dynamic-update-slice_fusion.24
  167.2 0.6 constant_dynamic-update-slice_fusion.23
  167.8 0.6 constant_dynamic-update-slice_fusion.22
  168.4 0.6 constant_dynamic-update-slice_fusion.21
  169.0 0.6 constant_dynamic-update-slice_fusion.20
  169.6 0.6 constant_dynamic-update-slice_fusion.19
  170.2 0.6 constant_dynamic-update-slice_fusion.18
  170.8 0.6 constant_dynamic-update-slice_fusion.17
  171.4 0.6 constant_dynamic-update-slice_fusion.16
  172.0 0.6 constant_dynamic-update-slice_fusion.15
  172.6 0.6 constant_dynamic-update-slice_fusion.14
  173.2 0.6 constant_dynamic-update-slice_fusion.13
  173.8 0.6 constant_dynamic-update-slice_fusion.12
  174.4 0.6 constant_dynamic-update-slice_fusion.11
  175.0 0.6 constant_dynamic-update-slice_fusion.10
  175.6 0.6 constant_dynamic-update-slice_fusion.9
  176.2 0.6 constant_dynamic-update-slice_fusion.8
  176.8 0.6 constant_dynamic-update-slice_fusion.7
  177.3 0.6 constant_dynamic-update-slice_fusion.6
  177.9 0.6 constant_dynamic-update-slice_fusion.5
  178.5 0.6 constant_dynamic-update-slice_fusion.4
  179.1 0.6 constant_dynamic-update-slice_fusion.3
  179.7 0.6 constant_dynamic-update-slice_fusion.2
  180.3 0.6 constant_dynamic-update-slice_fusion.1
  180.9 0.6 constant_dynamic-update-slice_fusion
  181.5 21.3 %all-to-all-start.4 = ((bf16[32,128,1,1,32]{1,4,3,2,0:T(8,128)(2,1)}), bf16[32,128,1,1,32]{1,4,3,2,0:T(8,128)(2,1)S(1)}, u32[]{:S(2)}, u32[]{:S(2)}) async-start(bf16[32,128,1,1,32]{1,4,3,2,0:T(8,128)(2,1)} %constant_dynamic-update-slice_fusion), calls=%async_computation.4 | async-start | bytes 524288 | tf_op jit(solution)/shard_map/all_to_all | solution.py:79
  202.9 0.1 reshape.80
  202.9 0.0 copy-done.5
  202.9 0.0 copy-done.6
  203.0 0.1 mul.28
  203.0 22.1 %all-to-all-done.4 = bf16[32,128,1,1,32]{1,4,3,2,0:T(8,128)(2,1)S(1)} async-done(((bf16[32,128,1,1,32]{1,4,3,2,0:T(8,128)(2,1)}), bf16[32,128,1,1,32]{1,4,3,2,0:T(8,128)(2,1)S(1)}, u32[]{:S(2)}, u32[]{:S(2)}) %all-to-all-start.4) | async-done | bytes 262176 | tf_op jit(solution)/shard_map/all_to_all | solution.py:79
  225.1 0.2 bitcast_multiply_fusion
  225.3 6.4 %scatter_custom_fusion = f32[128,128]{1,0:T(8,128)S(1)} fusion(s32[1024]{0:T(1024)S(1)} %bitcast.203, f32[128,1024]{0,1:T(8,128)S(1)} %bitcast_multiply_fusion, f32[]{:T(128)} %constant.11.clone.1), kind=kCustom, calls=%fused_computation.7 | custom fusion | flops 131072 | bytes 589828 | tf_op jit(solution)/shard_map/scatter-add | solution.py:88
  231.7 0.6 convert_element_type.34
  (9 shorter events, 0.1 us)
Async XLA Ops:
  0.0 1.6 copy-start
  43.3 55.3 %copy-start.2 = (bf16[1,2048,128]{2,1,0:T(8,128)(2,1)S(1)}, bf16[1,2048,128]{2,1,0:T(8,128)(2,1)}, u32[]{:S(2)}) copy-start(bf16[1,2048,128]{2,1,0:T(8,128)(2,1)} %param.9) | copy-start | bytes 1572868
  96.6 1.9 copy-start.1
  96.6 3.2 %copy-start.3 = (bf16[1,128,2048]{2,1,0:T(8,128)(2,1)S(1)}, bf16[1,128,2048]{2,1,0:T(8,128)(2,1)}, u32[]{:S(2)}) copy-start(bf16[1,128,2048]{2,1,0:T(8,128)(2,1)} %param.11) | copy-start | bytes 1572868
  96.6 3.2 %copy-start.4 = (bf16[1,2048,128]{2,1,0:T(8,128)(2,1)S(1)}, bf16[1,2048,128]{2,1,0:T(8,128)(2,1)}, u32[]{:S(2)}) copy-start(bf16[1,2048,128]{2,1,0:T(8,128)(2,1)} %param.10) | copy-start | bytes 1572868
  159.6 43.4 %copy-start.5 = (s32[32,32]{1,0:T(8,128)S(1)}, s32[32,32]{1,0:T(8,128)}, u32[]{:S(2)}) copy-start(s32[32,32]{1,0:T(8,128)} %param.7) | copy-start | bytes 12292
  159.6 43.4 %copy-start.6 = (f32[32,32]{1,0:T(8,128)S(1)}, f32[32,32]{1,0:T(8,128)}, u32[]{:S(2)}) copy-start(f32[32,32]{1,0:T(8,128)} %param.8) | copy-start | bytes 12292
  181.5 43.6 %all-to-all-start.4 = ((bf16[32,128,1,1,32]{1,4,3,2,0:T(8,128)(2,1)}), bf16[32,128,1,1,32]{1,4,3,2,0:T(8,128)(2,1)S(1)}, u32[]{:S(2)}, u32[]{:S(2)}) async-start(bf16[32,128,1,1,32]{1,4,3,2,0:T(8,128)(2,1)} %constant_dynamic-update-slice_fusion), calls=%async_computation.4 | async-start | bytes 524288 | tf_op jit(solution)/shard_map/all_to_all | solution.py:79
